TPU v7x, 32 devices: a whole 2x2x4 slice. The times are simulated.
32 devices in a mesh: sp: 8 (over z, x), tp: 4 (over y, core).
Axes of the slice: x: 2, y: 2, z: 4, core: 2. Of those that a mesh axis runs over, the one named last changes fastest.
Arguments:
- residual_in: bfloat16 [2048, 2048], P(('sp', 'tp')), may hold values from -0.119628906 to 0.119628906
- queries: bfloat16 [2048, 2048], P('sp', 'tp'), may hold values from -6 to 6
- keys_raw: bfloat16 [2048, 512], P('sp', 'tp'), may hold values from -6 to 6
- values_raw: bfloat16 [2048, 512], P('sp', 'tp'), may hold values from -6 to 6
- query_gain: float32 [128], replicated, may hold values from 0.28 to 7
- key_gain: float32 [128], replicated, may hold values from 0.28 to 7
- out_weight: bfloat16 [2048, 2048], P('tp'), may hold values from -0.125 to 0.125
- norm_gain: float32 [2048], replicated, may hold values from 0.1 to 1.9
- gate_weight: bfloat16 [2048, 5632], P('sp', 'tp'), may hold values from -0.125 to 0.125
- up_weight: bfloat16 [2048, 5632], P('sp', 'tp'), may hold values from -0.125 to 0.125
- down_weight: bfloat16 [5632, 2048], P('tp', 'sp'), may hold values from -0.078125 to 0.078125
Outputs:
- residual_out: bfloat16 [2048, 2048], P(('sp', 'tp'))
All inputs are finite; a program needn't handle non-finite values.
Results may differ from a plain program's by a relative error of at most 0.024.
The roundings to bfloat16 on the way count: a program that leaves them out, or rounds other values in their place, can miss the bound.
Values may be sent and summed in bfloat16 or wider, within the bound.
A program may use at most 128 MiB of HBM per device.

v0:
```python
import jax
import jax.numpy as jnp
from jax import lax
from jax.sharding import PartitionSpec as P

GRID_W = 64


EPS = 1e-06
THETA = 10000.0


def turn_half(part, angles):
    quarter = part.shape[-1] // 2
    cosine = jnp.cos(angles)[:, None, :]
    sine = jnp.sin(angles)[:, None, :]
    first = part[..., :quarter]
    second = part[..., quarter:]
    return part * cosine + jnp.concatenate([-second, first], axis=-1) * sine


def prepare_heads(raw, gain, positions, heads):
    count = raw.shape[0]
    head_dim = gain.shape[0]
    half = head_dim // 2
    vec = raw.astype(jnp.float32).reshape(count, heads, head_dim)
    vec = vec * lax.rsqrt(jnp.mean(vec * vec, axis=-1, keepdims=True) + EPS) * gain
    freqs = THETA ** (-jnp.arange(0, half, 2, dtype=jnp.float32) / half)
    row_ang = (positions // GRID_W).astype(jnp.float32)[:, None] * freqs
    col_ang = (positions % GRID_W).astype(jnp.float32)[:, None] * freqs
    row_ang = jnp.concatenate([row_ang, row_ang], axis=-1)
    col_ang = jnp.concatenate([col_ang, col_ang], axis=-1)
    turned = jnp.concatenate(
        [turn_half(vec[..., :half], row_ang), turn_half(vec[..., half:], col_ang)], axis=-1
    )
    return turned.astype(jnp.bfloat16)


def per_device(
    residual_in,
    queries,
    keys_raw,
    values_raw,
    query_gain,
    key_gain,
    out_weight,
    norm_gain,
    gate_weight,
    up_weight,
    down_weight,
):
    tok = queries.shape[0]
    head_dim = query_gain.shape[0]
    local_heads = queries.shape[1] // head_dim
    local_kv = keys_raw.shape[1] // head_dim
    group = local_heads // local_kv
    gate_full, up_full = (
        lax.all_gather(gate_weight, "sp", axis=0, tiled=True),
        lax.all_gather(up_weight, "sp", axis=0, tiled=True),
    )
    down_full = lax.all_gather(down_weight, "sp", axis=1, tiled=True)
    positions = lax.axis_index("sp") * tok + jnp.arange(tok, dtype=jnp.int32)
    q_rot = prepare_heads(queries, query_gain, positions, local_heads).reshape(
        tok, local_kv, group, head_dim
    )
    k_rot = prepare_heads(keys_raw, key_gain, positions, local_kv)
    vals = values_raw.reshape(tok, local_kv, head_dim)
    start_state = (
        jnp.full((tok, local_kv, group), -jnp.inf, jnp.float32),
        jnp.zeros((tok, local_kv, group), jnp.float32),
        jnp.zeros((tok, local_kv, group, head_dim), jnp.float32),
    )
    carry = start_state
    k_piece = lax.all_gather(k_rot, "sp", axis=0, tiled=True)
    v_piece = lax.all_gather(vals, "sp", axis=0, tiled=True)
    length = k_piece.shape[0]
    shards = length // tok
    per_step = max(1, 2048 // tok)
    factor = max((d for d in range(1, shards + 1) if shards % d == 0 and d <= per_step))
    span = factor * tok
    k_blocks = k_piece.reshape(length // span, span, local_kv, head_dim)
    v_blocks = v_piece.reshape(length // span, span, local_kv, head_dim)

    def step(state, blocks):
        top, total, summed = state
        k_blk, v_blk = blocks
        scores = jnp.einsum(
            "qkgd,skd->qkgs", q_rot, k_blk, preferred_element_type=jnp.float32
        ) * head_dim ** (-0.5)
        new_top = jnp.maximum(top, jnp.max(scores, axis=-1))
        shrink = jnp.exp(top - new_top)
        expo = jnp.exp(scores - new_top[..., None])
        total = total * shrink + jnp.sum(expo, axis=-1)
        summed = summed * shrink[..., None] + jnp.einsum(
            "qkgs,skd->qkgd", expo.astype(jnp.bfloat16), v_blk, preferred_element_type=jnp.float32
        )
        return ((new_top, total, summed), None)

    carry, _ = lax.scan(step, carry, (k_blocks, v_blocks))
    top, total, summed = carry
    attended = (summed / total[..., None]).astype(jnp.bfloat16).reshape(tok, local_heads * head_dim)
    projected = lax.psum_scatter(
        jnp.dot(attended, out_weight, preferred_element_type=jnp.float32).astype(jnp.bfloat16),
        "tp",
        scatter_dimension=0,
        tiled=True,
    ).astype(jnp.float32)
    mixed = (residual_in.astype(jnp.float32) + projected).astype(jnp.bfloat16)
    mixed_f = mixed.astype(jnp.float32)
    normed = (
        mixed_f * lax.rsqrt(jnp.mean(mixed_f * mixed_f, axis=-1, keepdims=True) + EPS) * norm_gain
    ).astype(jnp.bfloat16)
    whole_rows = lax.all_gather(normed, "tp", axis=0, tiled=True)
    gate = jnp.dot(whole_rows, gate_full, preferred_element_type=jnp.float32)
    up_val = jnp.dot(whole_rows, up_full, preferred_element_type=jnp.float32)
    hidden = (jax.nn.silu(gate) * up_val).astype(jnp.bfloat16)
    terms = jnp.dot(hidden, down_full, preferred_element_type=jnp.float32)
    fed = lax.psum_scatter(
        terms.astype(jnp.bfloat16), "tp", scatter_dimension=0, tiled=True
    ).astype(jnp.float32)
    return (mixed_f + 0.5 * fed).astype(jnp.bfloat16)


def solution(mesh):
    placed = (
        P(("sp", "tp"), None),
        P("sp", "tp"),
        P("sp", "tp"),
        P("sp", "tp"),
        P(),
        P(),
        P("tp", None),
        P(),
        P("sp", "tp"),
        P("sp", "tp"),
        P("tp", "sp"),
    )
    return jax.shard_map(
        per_device, mesh=mesh, in_specs=placed, out_specs=P(("sp", "tp"), None), check_vma=False
    )
```

profile of v0, /device:TPU:0, one launch (start us, length us, event | category | flops | bytes accessed | tf_op | source)
XLA Modules:
  0.0 460.9 jit_solution(13443270139341550448)
XLA Ops:
  6.5 0.0 copy-start
  6.5 0.0 reduce-scatter.3.cloned.1.call-start
  6.6 1.1 fusion.33
  7.7 0.9 fusion.35
  8.6 0.2 slice_negate_fusion.3
  8.8 0.8 broadcast_multiply_fusion.1
  9.6 1.2 fusion.39
  10.8 0.1 pad_maximum_fusion.4
  10.9 33.0 %all_gather.18 = bf16[2048,1,128]{2,0,1:T(8,128)(2,1)S(1)} all-gather(bf16[256,1,128]{2,0,1:T(8,128)(2,1)S(1)} %pad_maximum_fusion.4), channel_id=1, replica_groups=mesh['sp'=8,'tp'=4] {'sp'}, dimensions={0}, use_global_device_ids=true | all-gather | bytes 589824 | tf_op jit(solution)/shard_map/all_gather | solution.py:74
  43.9 1.1 copy.14
  45.0 0.1 multiply_reduce_fusion
  45.1 0.1 copy.15
  45.2 0.9 multiply_multiply_fusion
  46.1 0.5 slice_negate_fusion.1
  46.6 1.5 fusion.43
  48.1 0.5 fusion.41
  48.7 0.5 fusion.26
  49.1 1.3 bitcast_reduce_fusion
  50.5 0.0 copy-start.1
  50.5 0.0 copy-start.4
  50.5 3.2 copy-done.1
  53.7 1.4 fusion.1
  55.1 0.0 copy-done.4
  55.1 0.1 copy.16
  55.2 31.3 %all-gather = bf16[2048,128]{0,1:T(8,128)(2,1)S(1)} all-gather(bf16[256,128]{0,1:T(8,128)(2,1)S(1)} %copy.16), channel_id=2, replica_groups=mesh['sp'=8,'tp'=4] {'sp'}, dimensions={0}, use_global_device_ids=true | all-gather | bytes 589824 | tf_op jit(solution)/shard_map/all_gather | solution.py:75
  86.5 0.0 copy-start.2
  86.5 0.0 copy-start.5
  86.5 5.1 %fusion.16 = bf16[1,128,256,4]{2,1,3,0:T(8,128)(2,1)S(1)} fusion(f32[2048,256,4]{1,0,2:T(8,128)} %copy-done.1, f32[256,4]{0,1:T(4,128)S(1)} %get-tuple-element.50, bf16[2048,128]{0,1:T(8,128)(2,1)S(1)} %all-gather, f32[256,4]{0,1:T(4,128)S(1)} %get-tuple-element.43, f32[256,4]{0,1:T(4,128)S(1)} %get-tuple-element.42), kind=kOutput, calls=%fused_computation.14 | convolution fusion | flops 543555584 | bytes 9187328 | tf_op jit(solution)/shard_map/while/body/eval_jaxpr/qkgs,skd->qkgd/dot_general | solution.py:94
  91.6 0.0 copy-done
  91.6 1.7 convolution_convert_fusion
  93.3 0.0 reduce-scatter.3.cloned.1.call-update
  93.3 0.0 all-gather.6.cloned.1.call-start
  93.4 26.1 %reduce-scatter.3.cloned.1.call-done = bf16[64,2048]{1,0:T(8,128)(2,1)} async-done(((bf16[256,2048]{1,0:T(8,128)(2,1)}), bf16[64,2048]{1,0:T(8,128)(2,1)}) %reduce-scatter.3.cloned.1.call-update) | async-done | bytes 262160 | tf_op jit(solution)/shard_map/reduce_scatter | solution.py:102
  119.4 0.0 copy-done.2
  119.4 1.1 fusion.19
  120.6 0.0 copy-done.5
  120.6 1.8 fusion.21
  122.4 0.0 all-gather.6.cloned.1.call-update
  122.4 0.0 all-gather.8.cloned.1.call-start
  122.5 0.7 all-gather.8.cloned.1.call-update
  123.1 0.0 all-gather.10.cloned.1.call-start
  123.2 0.5 all-gather.10.cloned.1.call-update
  123.7 0.0 all-gather.12.cloned.1.call-start
  123.8 0.5 all-gather.12.cloned.1.call-update
  124.3 0.2 reduce-scatter.5.cloned.1.call-start
  124.5 14.7 %all-gather.6.cloned.1.call-done = bf16[256,2048]{1,0:T(8,128)(2,1)} async-done(((bf16[64,2048]{1,0:T(8,128)(2,1)}), bf16[256,2048]{1,0:T(8,128)(2,1)}) %all-gather.6.cloned.1.call-update) | async-done | bytes 1048592 | tf_op jit(solution)/shard_map/all_gather | solution.py:113
  139.3 94.5 %all-gather.8.cloned.1.call-done = bf16[2048,1408]{1,0:T(8,128)(2,1)} async-done(((bf16[256,1408]{1,0:T(8,128)(2,1)}), bf16[2048,1408]{1,0:T(8,128)(2,1)}) %all-gather.8.cloned.1.call-update) | async-done | bytes 5767184 | tf_op jit(solution)/shard_map/all_gather | solution.py:58
  233.8 5.9 %fusion.53 = f32[256,1408]{1,0:T(8,128)} fusion(bf16[256,2048]{1,0:T(8,128)(2,1)} %all-gather.6.cloned.1.call-done, bf16[2048,1408]{1,0:T(8,128)(2,1)} %all-gather.8.cloned.1.call-done), kind=kOutput, calls=%fused_computation.88 | convolution fusion | flops 1476395008 | bytes 8257536 | tf_op jit(solution)/shard_map/dot_general | solution.py:114
  239.7 0.0 copy-start.3
  239.7 86.7 %all-gather.10.cloned.1.call-done = bf16[2048,1408]{1,0:T(8,128)(2,1)} async-done(((bf16[256,1408]{1,0:T(8,128)(2,1)}), bf16[2048,1408]{1,0:T(8,128)(2,1)}) %all-gather.10.cloned.1.call-update) | async-done | bytes 5767184 | tf_op jit(solution)/shard_map/all_gather | solution.py:59
  326.3 93.2 %all-gather.12.cloned.1.call-done = bf16[1408,2048]{1,0:T(8,128)(2,1)} async-done(((bf16[1408,256]{1,0:T(8,128)(2,1)}), bf16[1408,2048]{1,0:T(8,128)(2,1)}) %all-gather.12.cloned.1.call-update) | async-done | bytes 5767184 | tf_op jit(solution)/shard_map/all_gather | solution.py:61
  419.6 9.5 %convolution_convert_fusion.1 = bf16[256,2048]{1,0:T(8,128)(2,1)} fusion(bf16[1408,2048]{1,0:T(8,128)(2,1)} %all-gather.12.cloned.1.call-done, bf16[256,2048]{1,0:T(8,128)(2,1)} %all-gather.6.cloned.1.call-done, bf16[2048,1408]{1,0:T(8,128)(2,1)} %all-gather.10.cloned.1.call-done, f32[256,1408]{1,0:T(8,128)} %fusion.53), kind=kOutput, calls=%fused_computation.10 | convolution fusion | flops 2955476992 | bytes 15073280 | tf_op jit(solution)/shard_map/dot_general | solution.py:117
  429.1 0.0 reduce-scatter.5.cloned.1.call-update
  429.1 23.1 %reduce-scatter.5.cloned.1.call-done = bf16[64,2048]{1,0:T(8,128)(2,1)} async-done(((bf16[256,2048]{1,0:T(8,128)(2,1)}), bf16[64,2048]{1,0:T(8,128)(2,1)}) %reduce-scatter.5.cloned.1.call-update) | async-done | bytes 262160 | tf_op jit(solution)/shard_map/reduce_scatter | solution.py:118
  452.3 0.0 copy-done.3
  452.3 1.8 fusion.22
  (6 shorter events, 0.1 us)
Async XLA Ops:
  6.5 85.0 %copy-start = (bf16[512,2048]{1,0:T(8,128)(2,1)S(1)}, bf16[512,2048]{1,0:T(8,128)(2,1)}, u32[]{:S(2)}) copy-start(bf16[512,2048]{1,0:T(8,128)(2,1)} %param.17) | copy-start | bytes 6291460
  6.5 112.9 %reduce-scatter.3.cloned.1.call-start = ((), (), s32[]{:S(2)}) async-start(), calls=%async_computation.2 | async-start | bytes 1310720 | tf_op jit(solution)/shard_map/reduce_scatter | solution.py:102
  50.5 3.2 copy-start.1
  50.5 4.6 %copy-start.4 = (bf16[256,128]{1,0:T(8,128)(2,1)S(1)}, bf16[256,128]{1,0:T(8,128)(2,1)}, u32[]{:S(2)}) copy-start(bf16[256,128]{1,0:T(8,128)(2,1)} %param.14) | copy-start | bytes 196612
  86.5 32.9 %copy-start.2 = (bf16[64,2048]{1,0:T(8,128)(2,1)S(1)}, bf16[64,2048]{1,0:T(8,128)(2,1)}, u32[]{:S(2)}) copy-start(bf16[64,2048]{1,0:T(8,128)(2,1)} %param.11) | copy-start | bytes 786436
  86.5 34.1 %copy-start.5 = (f32[2048]{0:T(1024)S(1)}, f32[2048]{0:T(1024)}, u32[]{:S(2)}) copy-start(f32[2048]{0:T(1024)} %param.18) | copy-start | bytes 24580
  93.3 45.9 %all-gather.6.cloned.1.call-start = ((), (), s32[]{:S(2)}) async-start(), calls=%async_computation.3 | async-start | bytes 1310720 | tf_op jit(solution)/shard_map/all_gather | solution.py:113
  122.4 111.4 %all-gather.8.cloned.1.call-start = ((), (), s32[]{:S(2)}) async-start(), calls=%async_computation.4 | async-start | bytes 6488064 | tf_op jit(solution)/shard_map/all_gather | solution.py:58
  123.1 203.2 %all-gather.10.cloned.1.call-start = ((), (), s32[]{:S(2)}) async-start(), calls=%async_computation.5 | async-start | bytes 6488064 | tf_op jit(solution)/shard_map/all_gather | solution.py:59
  123.7 295.9 %all-gather.12.cloned.1.call-start = ((), (), s32[]{:S(2)}) async-start(), calls=%async_computation.6 | async-start | bytes 6488064 | tf_op jit(solution)/shard_map/all_gather | solution.py:61
  124.3 327.9 %reduce-scatter.5.cloned.1.call-start = ((), (), s32[]{:S(2)}) async-start(), calls=%async_computation.7 | async-start | bytes 1310720 | tf_op jit(solution)/shard_map/reduce_scatter | solution.py:118
  239.7 212.6 %copy-start.3 = (bf16[64,2048]{1,0:T(8,128)(2,1)S(1)}, bf16[64,2048]{1,0:T(8,128)(2,1)}, u32[]{:S(2)}) copy-start(bf16[64,2048]{1,0:T(8,128)(2,1)} %reduce-scatter.3.cloned.1.call-done) | copy-start | bytes 786436
Sparse Core Ops, SparseCore 0:
  93.4 25.9 reduce-scatter.2
  122.5 16.6 all-gather.5
  141.4 92.2 all-gather.7
  235.8 90.4 all-gather.9
  328.2 91.2 all-gather.11
  429.2 22.9 reduce-scatter.4
where the time goes:
time: 461 us
  waiting for transfers between devices  340 us (74%)
  blocking collectives  64.3 us (14%)
  matrix products  23.5 us (5%)
  other arithmetic  14.3 us (3%)
  between operations  13.6 us (3%)
    all_gather x1, waiting for transfers between devices, per_device(): lax.all_gather(gate_weight, 'sp', axis=0, tiled=True)  94.5 us
    all_gather x1, waiting for transfers between devices, per_device(): down_full = lax.all_gather(down_weight, 'sp', axis=1, tiled=True)  93.2 us
    all_gather x1, waiting for transfers between devices, per_device(): lax.all_gather(up_weight, 'sp', axis=0, tiled=True)  86.7 us
    all_gather x1, blocking collectives, per_device(): k_piece = lax.all_gather(k_rot, 'sp', axis=0, tiled=True)  33 us
    all_gather x1, blocking collectives, per_device(): v_piece = lax.all_gather(vals, 'sp', axis=0, tiled=True)  31.3 us
    reduce_scatter x1, waiting for transfers between devices, per_device(): lax.psum_scatter(jnp.dot(attended, out_weight, preferred_element_type=jnp...  26.1 us
    reduce_scatter x1, waiting for transfers between devices, per_device(): lax.psum_scatter(terms.astype(jnp.bfloat16), 'tp', scatter_dimension=0, t...  23.1 us
    all_gather x1, waiting for transfers between devices, per_device(): whole_rows = lax.all_gather(normed, 'tp', axis=0, tiled=True)  14.7 us
  transfers between devices with their start and end apart: 6, of which 6 were waited for; matrix products, arithmetic and copies ran while one was open for 1% of the time, Pallas kernels for 0%

commit v1 on v0

--- a/solution.py
+++ b/solution.py
@@ -1,6 +1,9 @@
 import jax
 import jax.numpy as jnp
 from jax import lax
+from jax.experimental import pallas as pl
+from jax.experimental.pallas import tpu as pltpu
+import functools
 from jax.sharding import PartitionSpec as P
 
 GRID_W = 64
@@ -36,7 +39,7 @@
     return turned.astype(jnp.bfloat16)
 
 
-def per_device(
+def plain_device(
     residual_in,
     queries,
     keys_raw,
@@ -121,7 +124,350 @@
     return (mixed_f + 0.5 * fed).astype(jnp.bfloat16)
 
 
+NX = 2
+NC = 2
+LANES = 128
+
+
+def ring_kernel(
+    nz,
+    res_ref, q_ref, k_ref, v_ref, cos_ref, sin_ref, qg_ref, kg_ref, ow_ref, ng_ref, g_ref, u_ref, d_ref,
+    out_ref,
+    k_own, k_all, v_all, g_all, u_all, d_all, q_s, att_s, proj, proj_in, normed_all,
+    part, core_in, y_out, y_in, z_out, z_in, mixed_s,
+    kz_s, kz_r, kx_s, kx_r, wz_s, wz_r, wx_s, wx_r, pj_s, pj_r,
+    nz_s, nz_r, ny_s, ny_r, nc_s, nc_r, nf_s, nf_r,
+    c_s, c_r, y_s, y_r, z_s, z_r,
+):
+    f32, bf16 = jnp.float32, jnp.bfloat16
+    sp, tp = lax.axis_index("sp"), lax.axis_index("tp")
+    z, x = sp // NX, sp % NX
+    y, c = tp // NC, tp % NC
+    ntp = 2 * NC
+    tok = q_ref.shape[0]
+    hd = k_ref.shape[1]
+    heads = q_ref.shape[1] // hd
+    rows = res_ref.shape[0]
+    wide = res_ref.shape[1]
+    drows = g_ref.shape[0]
+    unit = g_all.shape[1]
+
+    def at_z(zz):
+        return (zz * NX + x, tp)
+
+    x_peer = (z * NX + (1 - x), tp)
+    y_peer = (sp, (1 - y) * NC + c)
+    c_peer = (sp, y * NC + (1 - c))
+
+    def up(d):
+        return lax.rem(z + d, nz)
+
+    def down(d):
+        return lax.rem(z + nz - d, nz)
+
+    def rc(src, dst, ss, rs, dev):
+        return pltpu.make_async_remote_copy(
+            src_ref=src, dst_ref=dst, send_sem=ss, recv_sem=rs, device_id=dev,
+            device_id_type=pl.DeviceIdType.MESH,
+        )
+
+    barrier = pltpu.get_barrier_semaphore()
+    peers = [at_z(up(d)) for d in range(1, nz)] + [x_peer]
+    peers += [(sp, lax.rem(tp + e, ntp)) for e in range(1, ntp)]
+    for dev in peers:
+        pl.semaphore_signal(barrier, inc=1, device_id=dev, device_id_type=pl.DeviceIdType.MESH)
+    pl.semaphore_wait(barrier, len(peers))
+
+    lane = lax.broadcasted_iota(jnp.int32, (tok, hd), 1)
+    low = (lane % (hd // 2)) < (hd // 4)
+    cosine, sine = cos_ref[...], sin_ref[...]
+
+    def prepare(raw, gain):
+        vec = raw.astype(f32)
+        vec = vec * lax.rsqrt(jnp.mean(vec * vec, axis=-1, keepdims=True) + EPS) * gain
+        swapped = jnp.where(low, pltpu.roll(vec, hd - hd // 4, 1), pltpu.roll(vec, hd // 4, 1))
+        return (vec * cosine + swapped * sine).astype(bf16)
+
+    def tok_rows(s):
+        return pl.ds(pl.multiple_of(s * tok, tok), tok)
+
+    def w_rows(s):
+        return pl.ds(pl.multiple_of(s * drows, drows), drows)
+
+    def w_cols(zz):
+        return pl.ds(pl.multiple_of(zz * unit, unit), unit)
+
+    k_new = prepare(k_ref[...], kg_ref[...])
+    k_own[...] = k_new
+    mine = tok_rows(sp)
+    k_all[mine, :] = k_new
+    v_all[mine, :] = v_ref[...]
+
+    kz = []
+    for d in range(1, nz):
+        kz.append((
+            rc(k_own, k_all.at[mine, :], kz_s.at[0, d], kz_r.at[0, d], at_z(up(d))),
+            rc(v_ref, v_all.at[mine, :], kz_s.at[1, d], kz_r.at[1, d], at_z(up(d))),
+        ))
+        for op in kz[-1]:
+            op.start()
+    kx = [(
+        rc(k_own, k_all.at[mine, :], kx_s.at[0, 0], kx_r.at[0, 0], x_peer),
+        rc(v_ref, v_all.at[mine, :], kx_s.at[1, 0], kx_r.at[1, 0], x_peer),
+    )]
+    for op in kx[0]:
+        op.start()
+
+    def pieces(zz, s_sem, r_sem, i, dev):
+        return (
+            rc(g_ref.at[:, w_cols(zz)], g_all.at[w_rows(sp), :], s_sem.at[0, i], r_sem.at[0, i], dev),
+            rc(u_ref.at[:, w_cols(zz)], u_all.at[w_rows(sp), :], s_sem.at[1, i], r_sem.at[1, i], dev),
+            rc(d_ref.at[w_cols(zz), :], d_all.at[sp], s_sem.at[2, i], r_sem.at[2, i], dev),
+        )
+
+    wz = []
+    for d in range(1, nz):
+        wz.append(pieces(up(d), wz_s, wz_r, d, at_z(up(d))))
+        for op in wz[-1]:
+            op.start()
+
+    for h in range(heads):
+        q_s[h] = prepare(q_ref[:, h * hd:(h + 1) * hd], qg_ref[...])
+    g_all[w_rows(sp), :] = g_ref[:, w_cols(z)]
+    u_all[w_rows(sp), :] = u_ref[:, w_cols(z)]
+    d_all[sp] = d_ref[w_cols(z), :]
+
+    for d in range(1, nz):
+        for op in kz[d - 1]:
+            op.wait_recv()
+        theirs = tok_rows(down(d) * NX + x)
+        kx.append((
+            rc(k_all.at[theirs, :], k_all.at[theirs, :], kx_s.at[0, d], kx_r.at[0, d], x_peer),
+            rc(v_all.at[theirs, :], v_all.at[theirs, :], kx_s.at[1, d], kx_r.at[1, d], x_peer),
+        ))
+        for op in kx[-1]:
+            op.start()
+    wx = [pieces(z, wx_s, wx_r, 0, x_peer)]
+    for op in wx[0]:
+        op.start()
+    for pair in kx:
+        for op in pair:
+            op.wait_recv()
+
+    scale = hd ** (-0.5)
+    for h in range(heads):
+        scores = lax.dot_general(
+            q_s[h], k_all[...], (((1,), (1,)), ((), ())), preferred_element_type=f32
+        )
+        top = jnp.max(scores, axis=-1, keepdims=True)
+        expo = jnp.exp((scores - top) * scale)
+        total = jnp.sum(expo, axis=-1, keepdims=True)
+        summed = jnp.dot(expo.astype(bf16), v_all[...], preferred_element_type=f32)
+        att_s[:, h * hd:(h + 1) * hd] = (summed / total).astype(bf16)
+
+    step = wide // 4
+    for i in range(4):
+        cols = slice(i * step, (i + 1) * step)
+        prod = jnp.dot(att_s[...], ow_ref[:, cols], preferred_element_type=f32)
+        proj[:, :, cols] = prod.astype(bf16).reshape(ntp, rows, step)
+    pj = []
+    for e in range(1, ntp):
+        to = lax.rem(tp + e, ntp)
+        pj.append(rc(proj.at[to], proj_in.at[e - 1], pj_s.at[e], pj_r.at[e], (sp, to)))
+        pj[-1].start()
+
+    def forward_weights(d):
+        for op in wz[d - 1]:
+            op.wait_recv()
+        s = down(d) * NX + x
+        wx.append((
+            rc(g_all.at[w_rows(s), :], g_all.at[w_rows(s), :], wx_s.at[0, d], wx_r.at[0, d], x_peer),
+            rc(u_all.at[w_rows(s), :], u_all.at[w_rows(s), :], wx_s.at[1, d], wx_r.at[1, d], x_peer),
+            rc(d_all.at[s], d_all.at[s], wx_s.at[2, d], wx_r.at[2, d], x_peer),
+        ))
+        for op in wx[-1]:
+            op.start()
+
+    for op in pj:
+        op.wait_recv()
+    projected = proj[tp].astype(f32)
+    for e in range(1, ntp):
+        projected = projected + proj_in[e - 1].astype(f32)
+    mixed = (res_ref[...].astype(f32) + projected).astype(bf16)
+    mixed_s[...] = mixed
+    mixed_f = mixed.astype(f32)
+    normed = (
+        mixed_f * lax.rsqrt(jnp.mean(mixed_f * mixed_f, axis=-1, keepdims=True) + EPS) * ng_ref[...]
+    ).astype(bf16)
+    own = z * ntp + tp
+    normed_all[own] = normed
+
+    nz_ops, ny_ops, nc_ops, nf_ops = [], [], [], []
+
+    def pass_on(d):
+        b = down(d) * ntp + tp
+        blk = normed_all.at[b]
+        ny_ops.append(rc(blk, blk, ny_s.at[d], ny_r.at[d], y_peer))
+        nc_ops.append(rc(blk, blk, nc_s.at[d], nc_r.at[d], c_peer))
+        ny_ops[-1].start()
+        nc_ops[-1].start()
+
+    def pass_over(d):
+        ny_ops[d].wait_recv()
+        blk = normed_all.at[down(d) * ntp + (1 - y) * NC + c]
+        nf_ops.append(rc(blk, blk, nf_s.at[d], nf_r.at[d], c_peer))
+        nf_ops[-1].start()
+
+    for d in range(1, nz):
+        blk = normed_all.at[own]
+        nz_ops.append(rc(blk, blk, nz_s.at[d], nz_r.at[d], at_z(up(d))))
+        nz_ops[-1].start()
+    pass_on(0)
+    for d in range(1, nz):
+        forward_weights(d)
+    pass_over(0)
+    for d in range(1, nz):
+        nz_ops[d - 1].wait_recv()
+        pass_on(d)
+    for d in range(1, nz):
+        pass_over(d)
+    for ops in wx:
+        for op in ops:
+            op.wait_recv()
+    for op in nc_ops + nf_ops:
+        op.wait_recv()
+
+    def core_ops(d, j):
+        b = up(d) * ntp + j * NC + (1 - c)
+        return rc(part.at[b], core_in.at[d, j], c_s.at[d, j], c_r.at[d, j], c_peer)
+
+    cols_each = d_all.shape[2]
+
+    def tile(i, carry):
+        d = lax.rem(i + 1, nz)
+        t = up(d)
+        x_t = normed_all[pl.ds(t * ntp, ntp)].reshape(ntp * rows, wide)
+        gate = jnp.dot(x_t, g_all[...], preferred_element_type=f32)
+        up_val = jnp.dot(x_t, u_all[...], preferred_element_type=f32)
+        hidden = (gate / (1.0 + jnp.exp(-gate)) * up_val).astype(bf16)
+        for s in range(d_all.shape[0]):
+            r = jnp.dot(hidden, d_all[s], preferred_element_type=f32).astype(bf16)
+            part[pl.ds(t * ntp, ntp), :, s * cols_each:(s + 1) * cols_each] = r.reshape(ntp, rows, cols_each)
+        for j in range(2):
+            core_ops(d, j).start()
+        return carry
+
+    lax.fori_loop(0, nz, tile, 0)
+
+    y_ops = {}
+    order = list(range(1, nz)) + [0]
+    for d in order:
+        for j in range(2):
+            core_ops(d, j).wait_recv()
+        b = up(d) * ntp + (1 - y) * NC + c
+        y_out[d] = (part[b].astype(f32) + core_in[d, 1 - y].astype(f32)).astype(bf16)
+        y_ops[d] = rc(y_out.at[d], y_in.at[d], y_s.at[d], y_r.at[d], y_peer)
+        y_ops[d].start()
+
+    def summed_tile(d):
+        b = up(d) * ntp + tp
+        return part[b].astype(f32) + core_in[d, y].astype(f32) + y_in[d].astype(f32)
+
+    z_ops = []
+    for d in range(1, nz):
+        y_ops[d].wait_recv()
+        z_out[d - 1] = summed_tile(d).astype(bf16)
+        z_ops.append(rc(z_out.at[d - 1], z_in.at[d - 1], z_s.at[d], z_r.at[d], at_z(up(d))))
+        z_ops[-1].start()
+    y_ops[0].wait_recv()
+    fed = summed_tile(0)
+    for d in range(1, nz):
+        z_ops[d - 1].wait_recv()
+        fed = fed + z_in[d - 1].astype(f32)
+    out_ref[...] = (mixed_s[...].astype(f32) + 0.5 * fed).astype(bf16)
+
+    for ops in kz + kx + wz + wx:
+        for op in ops:
+            op.wait_send()
+    for op in pj + nz_ops + ny_ops + nc_ops + nf_ops + z_ops + [y_ops[d] for d in order]:
+        op.wait_send()
+    for d in order:
+        for j in range(2):
+            core_ops(d, j).wait_send()
+
+
+def ring_device(
+    nsp,
+    residual_in, queries, keys_raw, values_raw, query_gain, key_gain, out_weight, norm_gain,
+    gate_weight, up_weight, down_weight,
+):
+    bf16 = jnp.bfloat16
+    nz = nsp // NX
+    tok = queries.shape[0]
+    hd = query_gain.shape[0]
+    heads = queries.shape[1] // hd
+    rows, wide = residual_in.shape
+    drows, units = gate_weight.shape
+    ntp = tok // rows
+    unit = -(-units // (nz * LANES)) * LANES
+    extra = nz * unit - units
+    gate_p = jnp.pad(gate_weight, ((0, 0), (0, extra)))
+    up_p = jnp.pad(up_weight, ((0, 0), (0, extra)))
+    down_p = jnp.pad(down_weight, ((0, extra), (0, 0)))
+    half = hd // 2
+    positions = lax.axis_index("sp") * tok + jnp.arange(tok, dtype=jnp.int32)
+    freqs = THETA ** (-jnp.arange(0, half, 2, dtype=jnp.float32) / half)
+    row_ang = (positions // GRID_W).astype(jnp.float32)[:, None] * freqs
+    col_ang = (positions % GRID_W).astype(jnp.float32)[:, None] * freqs
+    angles = jnp.concatenate([row_ang, row_ang, col_ang, col_ang], axis=-1)
+    sign = jnp.where(jnp.arange(hd) % half < half // 2, -1.0, 1.0)
+    cosine, sine = jnp.cos(angles), jnp.sin(angles) * sign
+    dma = pltpu.SemaphoreType.DMA
+    vm = pltpu.VMEM
+    blk = (rows, wide)
+    scratch = [
+        vm((tok, hd), bf16), vm((nsp * tok, hd), bf16), vm((nsp * tok, hd), bf16),
+        vm((nsp * drows, unit), bf16), vm((nsp * drows, unit), bf16), vm((nsp, unit, down_weight.shape[1]), bf16),
+        vm((heads, tok, hd), bf16), vm((tok, heads * hd), bf16),
+        vm((ntp,) + blk, bf16), vm((ntp - 1,) + blk, bf16), vm((nz * ntp,) + blk, bf16),
+        vm((nz * ntp,) + blk, bf16), vm((nz, 2) + blk, bf16), vm((nz,) + blk, bf16), vm((nz,) + blk, bf16),
+        vm((nz - 1,) + blk, bf16), vm((nz - 1,) + blk, bf16), vm(blk, bf16),
+        dma((2, nz)), dma((2, nz)), dma((2, nz)), dma((2, nz)),
+        dma((3, nz)), dma((3, nz)), dma((3, nz)), dma((3, nz)),
+        dma((ntp,)), dma((ntp,)),
+    ] + [dma((nz,)) for _ in range(8)] + [
+        dma((nz, 2)), dma((nz, 2)), dma((nz,)), dma((nz,)), dma((nz,)), dma((nz,)),
+    ]
+    return pl.pallas_call(
+        functools.partial(ring_kernel, nz),
+        out_shape=jax.ShapeDtypeStruct(blk, bf16),
+        in_specs=[pl.BlockSpec(memory_space=pltpu.VMEM)] * 13,
+        out_specs=pl.BlockSpec(memory_space=pltpu.VMEM),
+        scratch_shapes=scratch,
+        compiler_params=pltpu.CompilerParams(
+            collective_id=0, has_side_effects=True, vmem_limit_bytes=60 * 1024 * 1024
+        ),
+    )(
+        residual_in, queries, keys_raw, values_raw, cosine, sine, query_gain[None], key_gain[None],
+        out_weight, norm_gain[None], gate_p, up_p, down_p,
+    )
+
+
 def solution(mesh):
+    nsp, ntp = mesh.shape["sp"], mesh.shape["tp"]
+
+    def per_device(*arrays):
+        residual_in, queries, keys_raw = arrays[:3]
+        hd = arrays[4].shape[0]
+        small = (
+            nsp == 8 and ntp == 2 * NC and keys_raw.shape[1] == hd
+            and queries.shape[0] == ntp * residual_in.shape[0]
+            and arrays[8].shape[0] % LANES == 0 and queries.shape[0] <= 256
+        )
+        if small:
+            return ring_device(nsp, *arrays)
+        return plain_device(*arrays)
+
     placed = (
         P(("sp", "tp"), None),
         P("sp", "tp"),

time: 461 us -> 155 us (0.34)
  the two profiles are of different devices: /device:TPU:0 before, /device:TPU:9 now
where the time goes in v1:
time: 155 us
  Pallas kernels  147 us (95%)
  local copies, waits for them, and re-layouts  5.64 us (4%)
    pallas_call x1, Pallas kernels, ring_device(): pl.pallas_call(functools.partial(ring_kernel, nz), out_shape=jax.ShapeDty...  147 us

profile of v1, /device:TPU:9, one launch (start us, length us, event | category | flops | bytes accessed | tf_op | source)
XLA Modules:
  0.0 154.6 jit_solution(17260728289424610566)
XLA Ops:
  0.0 0.0 copy-start.1
  0.0 0.0 copy-start
  0.0 0.1 broadcast_multiply_fusion.1
  0.2 1.3 sine_multiply_fusion
  1.5 2.1 %pad.11.g_ref = bf16[256,1536]{1,0:T(8,128)(2,1)} pad(bf16[256,1408]{1,0:T(8,128)(2,1)} %param.19, bf16[]{:T(256)} %constant.60.clone.1), padding=0_0x0_128 | pad | bytes 1507330 | tf_op jit(solution)/shard_map/jit(_pad)/pad | solution.py:414
  3.5 0.0 copy-done
  3.5 1.0 pad.12.u_ref
  4.5 0.0 copy-done.1
  4.5 1.0 pad.13.d_ref
  5.4 147.5 %shard_map.109 = bf16[64,2048]{1,0:T(8,128)(2,1)} custom-call(bf16[64,2048]{1,0:T(8,128)(2,1)} %res_ref.1, bf16[256,512]{1,0:T(8,128)(2,1)} %q_ref.1, bf16[256,128]{1,0:T(8,128)(2,1)} %k_ref.1, bf16[256,128]{1,0:T(8,128)(2,1)} %v_ref.1, f32[256,128]{1,0:T(8,128)} %get-tuple-element.6.cos_ref, f32[256,128]{1,0:T(8,128)} %get-tuple-element.5.sin_ref, ...), custom_call_target="tpu_custom_call" | custom-call | tf_op jit(solution)/shard_map/pallas_call | solution.py:441
  152.9 1.7 %copy.13 = bf16[64,2048]{1,0:T(8,128)(2,1)} copy(bf16[64,2048]{1,0:T(8,128)(2,1)} %shard_map.109) | data formatting | bytes 524288
  (3 shorter events, 0.0 us)
Async XLA Ops:
  0.0 4.5 %copy-start.1 = (bf16[1408,256]{1,0:T(8,128)(2,1)S(1)}, bf16[1408,256]{1,0:T(8,128)(2,1)}, u32[]{:S(2)}) copy-start(bf16[1408,256]{1,0:T(8,128)(2,1)} %param.21) | copy-start | bytes 2162692
  0.0 3.5 %copy-start = (bf16[256,1408]{1,0:T(8,128)(2,1)S(1)}, bf16[256,1408]{1,0:T(8,128)(2,1)}, u32[]{:S(2)}) copy-start(bf16[256,1408]{1,0:T(8,128)(2,1)} %param.20) | copy-start | bytes 2162692

commit v2 on v1

--- a/solution.py
+++ b/solution.py
@@ -133,11 +133,11 @@
     nz,
     res_ref, q_ref, k_ref, v_ref, cos_ref, sin_ref, qg_ref, kg_ref, ow_ref, ng_ref, g_ref, u_ref, d_ref,
     out_ref,
-    k_own, k_all, v_all, g_all, u_all, d_all, q_s, att_s, proj, proj_in, normed_all,
+    g_own, u_own, d_own, k_own, k_all, v_all, g_all, u_all, d_all, q_s, att_s, proj, proj_in, normed_all,
     part, core_in, y_out, y_in, z_out, z_in, mixed_s,
     kz_s, kz_r, kx_s, kx_r, wz_s, wz_r, wx_s, wx_r, pj_s, pj_r,
     nz_s, nz_r, ny_s, ny_r, nc_s, nc_r, nf_s, nf_r,
-    c_s, c_r, y_s, y_r, z_s, z_r,
+    c_s, c_r, y_s, y_r, z_s, z_r, kf_s, af_s, ld_s,
 ):
     f32, bf16 = jnp.float32, jnp.bfloat16
     sp, tp = lax.axis_index("sp"), lax.axis_index("tp")
@@ -171,6 +171,26 @@
             device_id_type=pl.DeviceIdType.MESH,
         )
 
+    units = g_ref.shape[1]
+    loads = (
+        pltpu.make_async_copy(g_ref, g_own.at[:, pl.ds(0, units)], ld_s.at[0]),
+        pltpu.make_async_copy(u_ref, u_own.at[:, pl.ds(0, units)], ld_s.at[1]),
+        pltpu.make_async_copy(d_ref, d_own.at[pl.ds(0, units), :], ld_s.at[2]),
+    )
+    for op in loads:
+        op.start()
+    extra = g_own.shape[1] - units
+    if extra:
+        g_own[:, units:] = jnp.zeros((drows, extra), bf16)
+        u_own[:, units:] = jnp.zeros((drows, extra), bf16)
+        d_own[units:, :] = jnp.zeros((extra, d_own.shape[1]), bf16)
+
+    def near(i):
+        i = jnp.int32(i)
+        ahead = jnp.where(i == 1, 0, i)
+        inner = jnp.where(z == 1, ahead, nz - 1 - ahead)
+        return jnp.where(i == 0, z, jnp.where(z == 0, i, jnp.where(z == nz - 1, nz - 1 - i, inner)))
+
     barrier = pltpu.get_barrier_semaphore()
     peers = [at_z(up(d)) for d in range(1, nz)] + [x_peer]
     peers += [(sp, lax.rem(tp + e, ntp)) for e in range(1, ntp)]
@@ -203,14 +223,39 @@
     k_all[mine, :] = k_new
     v_all[mine, :] = v_ref[...]
 
-    kz = []
-    for d in range(1, nz):
-        kz.append((
-            rc(k_own, k_all.at[mine, :], kz_s.at[0, d], kz_r.at[0, d], at_z(up(d))),
-            rc(v_ref, v_all.at[mine, :], kz_s.at[1, d], kz_r.at[1, d], at_z(up(d))),
-        ))
-        for op in kz[-1]:
+    def line_dev(way):
+        return at_z(lax.clamp(0, z + way, nz - 1))
+
+    def onward(t):
+        way = jnp.where(t < z, 1, -1)
+        inside = jnp.logical_and(z + way >= 0, z + way < nz)
+        return at_z(lax.clamp(0, z + way, nz - 1)), inside
+
+    ways = ((1, z < nz - 1), (-1, z > 0))
+
+    def kv_out(w, way):
+        return (
+            rc(k_own, k_all.at[mine, :], kz_s.at[0, w], kz_r.at[0, z], line_dev(way)),
+            rc(v_ref, v_all.at[mine, :], kz_s.at[1, w], kz_r.at[1, z], line_dev(way)),
+        )
+
+    def kv_in(t, i, dev):
+        theirs = tok_rows(t * NX + x)
+        return (
+            rc(k_all.at[theirs, :], k_all.at[theirs, :], kf_s.at[0, i], kz_r.at[0, t], dev),
+            rc(v_all.at[theirs, :], v_all.at[theirs, :], kf_s.at[1, i], kz_r.at[1, t], dev),
+        )
+
+    def starts(ops):
+        for op in ops:
             op.start()
+
+    def sent(ops):
+        for op in ops:
+            op.wait_send()
+
+    for w, (way, ok) in enumerate(ways):
+        pl.when(ok)(functools.partial(starts, kv_out(w, way)))
     kx = [(
         rc(k_own, k_all.at[mine, :], kx_s.at[0, 0], kx_r.at[0, 0], x_peer),
         rc(v_ref, v_all.at[mine, :], kx_s.at[1, 0], kx_r.at[1, 0], x_peer),
@@ -220,11 +265,13 @@
 
     def pieces(zz, s_sem, r_sem, i, dev):
         return (
-            rc(g_ref.at[:, w_cols(zz)], g_all.at[w_rows(sp), :], s_sem.at[0, i], r_sem.at[0, i], dev),
-            rc(u_ref.at[:, w_cols(zz)], u_all.at[w_rows(sp), :], s_sem.at[1, i], r_sem.at[1, i], dev),
-            rc(d_ref.at[w_cols(zz), :], d_all.at[sp], s_sem.at[2, i], r_sem.at[2, i], dev),
-        )
-
+            rc(g_own.at[:, w_cols(zz)], g_all.at[w_rows(sp), :], s_sem.at[0, i], r_sem.at[0, i], dev),
+            rc(u_own.at[:, w_cols(zz)], u_all.at[w_rows(sp), :], s_sem.at[1, i], r_sem.at[1, i], dev),
+            rc(d_own.at[w_cols(zz), :], d_all.at[sp], s_sem.at[2, i], r_sem.at[2, i], dev),
+        )
+
+    for op in loads:
+        op.wait()
     wz = []
     for d in range(1, nz):
         wz.append(pieces(up(d), wz_s, wz_r, d, at_z(up(d))))
@@ -233,20 +280,23 @@
 
     for h in range(heads):
         q_s[h] = prepare(q_ref[:, h * hd:(h + 1) * hd], qg_ref[...])
-    g_all[w_rows(sp), :] = g_ref[:, w_cols(z)]
-    u_all[w_rows(sp), :] = u_ref[:, w_cols(z)]
-    d_all[sp] = d_ref[w_cols(z), :]
-
-    for d in range(1, nz):
-        for op in kz[d - 1]:
+    g_all[w_rows(sp), :] = g_own[:, w_cols(z)]
+    u_all[w_rows(sp), :] = u_own[:, w_cols(z)]
+    d_all[sp] = d_own[w_cols(z), :]
+
+    for i in range(1, nz):
+        t = near(i)
+        dev, inside = onward(t)
+        ops = kv_in(t, i, dev)
+        for op in ops:
             op.wait_recv()
-        theirs = tok_rows(down(d) * NX + x)
+        pl.when(inside)(functools.partial(starts, ops))
+        theirs = tok_rows(t * NX + x)
         kx.append((
-            rc(k_all.at[theirs, :], k_all.at[theirs, :], kx_s.at[0, d], kx_r.at[0, d], x_peer),
-            rc(v_all.at[theirs, :], v_all.at[theirs, :], kx_s.at[1, d], kx_r.at[1, d], x_peer),
+            rc(k_all.at[theirs, :], k_all.at[theirs, :], kx_s.at[0, i], kx_r.at[0, i], x_peer),
+            rc(v_all.at[theirs, :], v_all.at[theirs, :], kx_s.at[1, i], kx_r.at[1, i], x_peer),
         ))
-        for op in kx[-1]:
-            op.start()
+        starts(kx[-1])
     wx = [pieces(z, wx_s, wx_r, 0, x_peer)]
     for op in wx[0]:
         op.start()
@@ -288,6 +338,7 @@
         for op in wx[-1]:
             op.start()
 
+    forward_weights(1)
     for op in pj:
         op.wait_recv()
     projected = proj[tp].astype(f32)
@@ -302,50 +353,79 @@
     own = z * ntp + tp
     normed_all[own] = normed
 
-    nz_ops, ny_ops, nc_ops, nf_ops = [], [], [], []
-
-    def pass_on(d):
-        b = down(d) * ntp + tp
-        blk = normed_all.at[b]
-        ny_ops.append(rc(blk, blk, ny_s.at[d], ny_r.at[d], y_peer))
-        nc_ops.append(rc(blk, blk, nc_s.at[d], nc_r.at[d], c_peer))
-        ny_ops[-1].start()
-        nc_ops[-1].start()
-
-    def pass_over(d):
-        ny_ops[d].wait_recv()
-        blk = normed_all.at[down(d) * ntp + (1 - y) * NC + c]
-        nf_ops.append(rc(blk, blk, nf_s.at[d], nf_r.at[d], c_peer))
-        nf_ops[-1].start()
-
-    for d in range(1, nz):
-        blk = normed_all.at[own]
-        nz_ops.append(rc(blk, blk, nz_s.at[d], nz_r.at[d], at_z(up(d))))
-        nz_ops[-1].start()
-    pass_on(0)
-    for d in range(1, nz):
-        forward_weights(d)
-    pass_over(0)
-    for d in range(1, nz):
-        nz_ops[d - 1].wait_recv()
-        pass_on(d)
-    for d in range(1, nz):
-        pass_over(d)
+    mine_blk = normed_all.at[own]
+
+    def row_out(w, way):
+        return rc(mine_blk, mine_blk, nz_s.at[w], nz_r.at[z], line_dev(way))
+
+    def row_in(t, i, dev):
+        blk = normed_all.at[t * ntp + tp]
+        return rc(blk, blk, af_s.at[i], nz_r.at[t], dev)
+
+    def y_copy(t):
+        blk = normed_all.at[t * ntp + tp]
+        return rc(blk, blk, ny_s.at[t], ny_r.at[t], y_peer)
+
+    def c_copy(t):
+        blk = normed_all.at[t * ntp + tp]
+        return rc(blk, blk, nc_s.at[t], nc_r.at[t], c_peer)
+
+    def f_copy(t):
+        blk = normed_all.at[t * ntp + (1 - y) * NC + c]
+        return rc(blk, blk, nf_s.at[t], nf_r.at[t], c_peer)
+
+    def pass_on(t):
+        y_copy(t).start()
+        c_copy(t).start()
+
+    def pass_over(t):
+        y_copy(t).wait_recv()
+        f_copy(t).start()
+
+    for w, (way, ok) in enumerate(ways):
+        pl.when(ok)(row_out(w, way).start)
+    pass_on(z)
+    forward_weights(2)
+    pass_over(z)
+    forward_weights(3)
+    for i in range(1, nz):
+        t = near(i)
+        dev, inside = onward(t)
+        op = row_in(t, i, dev)
+        op.wait_recv()
+        pl.when(inside)(op.start)
+        pass_on(t)
+        if i > 1:
+            pass_over(near(i - 1))
     for ops in wx:
         for op in ops:
             op.wait_recv()
-    for op in nc_ops + nf_ops:
-        op.wait_recv()
-
-    def core_ops(d, j):
-        b = up(d) * ntp + j * NC + (1 - c)
-        return rc(part.at[b], core_in.at[d, j], c_s.at[d, j], c_r.at[d, j], c_peer)
+
+    def core_ops(t, j):
+        b = t * ntp + j * NC + (1 - c)
+        return rc(part.at[b], core_in.at[t, j], c_s.at[t, j], c_r.at[t, j], c_peer)
+
+    def y_op(t):
+        return rc(y_out.at[t], y_in.at[t], y_s.at[t], y_r.at[t], y_peer)
+
+    def y_stage(t):
+        for j in range(2):
+            core_ops(t, j).wait_recv()
+        b = t * ntp + (1 - y) * NC + c
+        y_out[t] = (part[b].astype(f32) + core_in[t, 1 - y].astype(f32)).astype(bf16)
+        y_op(t).start()
 
     cols_each = d_all.shape[2]
 
     def tile(i, carry):
-        d = lax.rem(i + 1, nz)
-        t = up(d)
+        t = near(i)
+
+        @pl.when(i == nz - 2)
+        def _():
+            pass_over(near(nz - 1))
+
+        c_copy(t).wait_recv()
+        f_copy(t).wait_recv()
         x_t = normed_all[pl.ds(t * ntp, ntp)].reshape(ntp * rows, wide)
         gate = jnp.dot(x_t, g_all[...], preferred_element_type=f32)
         up_val = jnp.dot(x_t, u_all[...], preferred_element_type=f32)
@@ -354,46 +434,50 @@
             r = jnp.dot(hidden, d_all[s], preferred_element_type=f32).astype(bf16)
             part[pl.ds(t * ntp, ntp), :, s * cols_each:(s + 1) * cols_each] = r.reshape(ntp, rows, cols_each)
         for j in range(2):
-            core_ops(d, j).start()
+            core_ops(t, j).start()
+
+        @pl.when(i > 1)
+        def _():
+            y_stage(near(i - 1))
+
         return carry
 
     lax.fori_loop(0, nz, tile, 0)
 
-    y_ops = {}
-    order = list(range(1, nz)) + [0]
-    for d in order:
-        for j in range(2):
-            core_ops(d, j).wait_recv()
-        b = up(d) * ntp + (1 - y) * NC + c
-        y_out[d] = (part[b].astype(f32) + core_in[d, 1 - y].astype(f32)).astype(bf16)
-        y_ops[d] = rc(y_out.at[d], y_in.at[d], y_s.at[d], y_r.at[d], y_peer)
-        y_ops[d].start()
-
-    def summed_tile(d):
-        b = up(d) * ntp + tp
-        return part[b].astype(f32) + core_in[d, y].astype(f32) + y_in[d].astype(f32)
-
-    z_ops = []
-    for d in range(1, nz):
-        y_ops[d].wait_recv()
-        z_out[d - 1] = summed_tile(d).astype(bf16)
-        z_ops.append(rc(z_out.at[d - 1], z_in.at[d - 1], z_s.at[d], z_r.at[d], at_z(up(d))))
-        z_ops[-1].start()
-    y_ops[0].wait_recv()
-    fed = summed_tile(0)
-    for d in range(1, nz):
-        z_ops[d - 1].wait_recv()
-        fed = fed + z_in[d - 1].astype(f32)
+    y_stage(near(nz - 1))
+    y_stage(z)
+
+    def summed_tile(t):
+        return part[t * ntp + tp].astype(f32) + core_in[t, y].astype(f32) + y_in[t].astype(f32)
+
+    def z_op(i):
+        return rc(z_out.at[i], z_in.at[z], z_s.at[i], z_r.at[z], at_z(near(i)))
+
+    for i in range(1, nz):
+        t = near(i)
+        y_op(t).wait_recv()
+        z_out[i] = summed_tile(t).astype(bf16)
+        z_op(i).start()
+    y_op(z).wait_recv()
+    fed = summed_tile(z)
+    for i in range(1, nz):
+        t = near(i)
+        rc(z_out.at[i], z_in.at[t], z_s.at[i], z_r.at[t], at_z(t)).wait_recv()
+        fed = fed + z_in[t].astype(f32)
     out_ref[...] = (mixed_s[...].astype(f32) + 0.5 * fed).astype(bf16)
 
-    for ops in kz + kx + wz + wx:
-        for op in ops:
-            op.wait_send()
-    for op in pj + nz_ops + ny_ops + nc_ops + nf_ops + z_ops + [y_ops[d] for d in order]:
-        op.wait_send()
-    for d in order:
-        for j in range(2):
-            core_ops(d, j).wait_send()
+    for ops in kx + wz + wx:
+        sent(ops)
+    sent(pj)
+    for w, (way, ok) in enumerate(ways):
+        pl.when(ok)(functools.partial(sent, kv_out(w, way) + (row_out(w, way),)))
+    for i in range(nz):
+        t = near(i)
+        sent((y_copy(t), c_copy(t), f_copy(t), core_ops(t, 0), core_ops(t, 1), y_op(t)))
+        if i:
+            dev, inside = onward(t)
+            pl.when(inside)(functools.partial(sent, kv_in(t, i, dev) + (row_in(t, i, dev),)))
+            z_op(i).wait_send()
 
 
 def ring_device(
@@ -410,10 +494,6 @@
     drows, units = gate_weight.shape
     ntp = tok // rows
     unit = -(-units // (nz * LANES)) * LANES
-    extra = nz * unit - units
-    gate_p = jnp.pad(gate_weight, ((0, 0), (0, extra)))
-    up_p = jnp.pad(up_weight, ((0, 0), (0, extra)))
-    down_p = jnp.pad(down_weight, ((0, extra), (0, 0)))
     half = hd // 2
     positions = lax.axis_index("sp") * tok + jnp.arange(tok, dtype=jnp.int32)
     freqs = THETA ** (-jnp.arange(0, half, 2, dtype=jnp.float32) / half)
@@ -426,22 +506,24 @@
     vm = pltpu.VMEM
     blk = (rows, wide)
     scratch = [
+        vm((drows, nz * unit), bf16), vm((drows, nz * unit), bf16), vm((nz * unit, down_weight.shape[1]), bf16),
         vm((tok, hd), bf16), vm((nsp * tok, hd), bf16), vm((nsp * tok, hd), bf16),
         vm((nsp * drows, unit), bf16), vm((nsp * drows, unit), bf16), vm((nsp, unit, down_weight.shape[1]), bf16),
         vm((heads, tok, hd), bf16), vm((tok, heads * hd), bf16),
         vm((ntp,) + blk, bf16), vm((ntp - 1,) + blk, bf16), vm((nz * ntp,) + blk, bf16),
         vm((nz * ntp,) + blk, bf16), vm((nz, 2) + blk, bf16), vm((nz,) + blk, bf16), vm((nz,) + blk, bf16),
-        vm((nz - 1,) + blk, bf16), vm((nz - 1,) + blk, bf16), vm(blk, bf16),
+        vm((nz,) + blk, bf16), vm((nz,) + blk, bf16), vm(blk, bf16),
         dma((2, nz)), dma((2, nz)), dma((2, nz)), dma((2, nz)),
         dma((3, nz)), dma((3, nz)), dma((3, nz)), dma((3, nz)),
         dma((ntp,)), dma((ntp,)),
     ] + [dma((nz,)) for _ in range(8)] + [
         dma((nz, 2)), dma((nz, 2)), dma((nz,)), dma((nz,)), dma((nz,)), dma((nz,)),
+        dma((2, nz)), dma((nz,)), dma((3,)),
     ]
     return pl.pallas_call(
         functools.partial(ring_kernel, nz),
         out_shape=jax.ShapeDtypeStruct(blk, bf16),
-        in_specs=[pl.BlockSpec(memory_space=pltpu.VMEM)] * 13,
+        in_specs=[pl.BlockSpec(memory_space=pltpu.VMEM)] * 10 + [pl.BlockSpec(memory_space=pl.ANY)] * 3,
         out_specs=pl.BlockSpec(memory_space=pltpu.VMEM),
         scratch_shapes=scratch,
         compiler_params=pltpu.CompilerParams(
@@ -449,7 +531,7 @@
         ),
     )(
         residual_in, queries, keys_raw, values_raw, cosine, sine, query_gain[None], key_gain[None],
-        out_weight, norm_gain[None], gate_p, up_p, down_p,
+        out_weight, norm_gain[None], gate_weight, up_weight, down_weight,
     )
 
 

time: 155 us -> 169 us (1.090)
  the two profiles are of different devices: /device:TPU:9 before, /device:TPU:0 now
where the time goes in v2:
time: 169 us; the launch traced here: 168 us
  Pallas kernels  165 us (98%)
    pallas_call x1, Pallas kernels, ring_device(): pl.pallas_call(functools.partial(ring_kernel, nz), out_shape=jax.ShapeDty...  165 us

profile of v2, /device:TPU:0, one launch (start us, length us, event | category | flops | bytes accessed | tf_op | source)
XLA Modules:
  0.0 168.4 jit_solution(10624348890643722359)
XLA Ops:
  0.0 0.1 broadcast_multiply_fusion.1
  0.2 1.3 sine_multiply_fusion
  1.4 165.3 %shard_map.109 = bf16[64,2048]{1,0:T(8,128)(2,1)} custom-call(bf16[64,2048]{1,0:T(8,128)(2,1)} %res_ref.1, bf16[256,512]{1,0:T(8,128)(2,1)} %q_ref.1, bf16[256,128]{1,0:T(8,128)(2,1)} %k_ref.1, bf16[256,128]{1,0:T(8,128)(2,1)} %v_ref.1, f32[256,128]{1,0:T(8,128)} %get-tuple-element.6.cos_ref, f32[256,128]{1,0:T(8,128)} %get-tuple-element.5.sin_ref, ...), custom_call_target="tpu_custom_call" | custom-call | tf_op jit(solution)/shard_map/pallas_call | solution.py:523
  166.7 1.7 copy.13
  (3 shorter events, 0.0 us)

commit v3 on v2

--- a/solution.py
+++ b/solution.py
@@ -137,7 +137,7 @@
     part, core_in, y_out, y_in, z_out, z_in, mixed_s,
     kz_s, kz_r, kx_s, kx_r, wz_s, wz_r, wx_s, wx_r, pj_s, pj_r,
     nz_s, nz_r, ny_s, ny_r, nc_s, nc_r, nf_s, nf_r,
-    c_s, c_r, y_s, y_r, z_s, z_r, kf_s, af_s, ld_s,
+    c_s, c_r, y_s, y_r, z_s, z_r, af_s, ld_s,
 ):
     f32, bf16 = jnp.float32, jnp.bfloat16
     sp, tp = lax.axis_index("sp"), lax.axis_index("tp")
@@ -233,17 +233,19 @@
 
     ways = ((1, z < nz - 1), (-1, z > 0))
 
-    def kv_out(w, way):
+    def kv_out(i):
+        dev = at_z(near(i))
         return (
-            rc(k_own, k_all.at[mine, :], kz_s.at[0, w], kz_r.at[0, z], line_dev(way)),
-            rc(v_ref, v_all.at[mine, :], kz_s.at[1, w], kz_r.at[1, z], line_dev(way)),
-        )
-
-    def kv_in(t, i, dev):
+            rc(k_own, k_all.at[mine, :], kz_s.at[0, i], kz_r.at[0, z], dev),
+            rc(v_ref, v_all.at[mine, :], kz_s.at[1, i], kz_r.at[1, z], dev),
+        )
+
+    def kv_in(i):
+        t = near(i)
         theirs = tok_rows(t * NX + x)
         return (
-            rc(k_all.at[theirs, :], k_all.at[theirs, :], kf_s.at[0, i], kz_r.at[0, t], dev),
-            rc(v_all.at[theirs, :], v_all.at[theirs, :], kf_s.at[1, i], kz_r.at[1, t], dev),
+            rc(k_own, k_all.at[theirs, :], kz_s.at[0, i], kz_r.at[0, t], at_z(t)),
+            rc(v_ref, v_all.at[theirs, :], kz_s.at[1, i], kz_r.at[1, t], at_z(t)),
         )
 
     def starts(ops):
@@ -254,8 +256,8 @@
         for op in ops:
             op.wait_send()
 
-    for w, (way, ok) in enumerate(ways):
-        pl.when(ok)(functools.partial(starts, kv_out(w, way)))
+    for i in range(nz - 1, 0, -1):
+        starts(kv_out(i))
     kx = [(
         rc(k_own, k_all.at[mine, :], kx_s.at[0, 0], kx_r.at[0, 0], x_peer),
         rc(v_ref, v_all.at[mine, :], kx_s.at[1, 0], kx_r.at[1, 0], x_peer),
@@ -286,11 +288,8 @@
 
     for i in range(1, nz):
         t = near(i)
-        dev, inside = onward(t)
-        ops = kv_in(t, i, dev)
-        for op in ops:
+        for op in kv_in(i):
             op.wait_recv()
-        pl.when(inside)(functools.partial(starts, ops))
         theirs = tok_rows(t * NX + x)
         kx.append((
             rc(k_all.at[theirs, :], k_all.at[theirs, :], kx_s.at[0, i], kx_r.at[0, i], x_peer),
@@ -470,13 +469,14 @@
         sent(ops)
     sent(pj)
     for w, (way, ok) in enumerate(ways):
-        pl.when(ok)(functools.partial(sent, kv_out(w, way) + (row_out(w, way),)))
+        pl.when(ok)(row_out(w, way).wait_send)
     for i in range(nz):
         t = near(i)
         sent((y_copy(t), c_copy(t), f_copy(t), core_ops(t, 0), core_ops(t, 1), y_op(t)))
         if i:
             dev, inside = onward(t)
-            pl.when(inside)(functools.partial(sent, kv_in(t, i, dev) + (row_in(t, i, dev),)))
+            pl.when(inside)(row_in(t, i, dev).wait_send)
+            sent(kv_out(i))
             z_op(i).wait_send()
 
 
@@ -518,7 +518,7 @@
         dma((ntp,)), dma((ntp,)),
     ] + [dma((nz,)) for _ in range(8)] + [
         dma((nz, 2)), dma((nz, 2)), dma((nz,)), dma((nz,)), dma((nz,)), dma((nz,)),
-        dma((2, nz)), dma((nz,)), dma((3,)),
+        dma((nz,)), dma((3,)),
     ]
     return pl.pallas_call(
         functools.partial(ring_kernel, nz),

time: 169 us -> 146 us (0.86)
  Pallas kernels: 165 us -> 143 us
    pallas_call x1, Pallas kernels: 165 us -> 143 us  [ring_device(): pl.pallas_call(functools.partial(ring_kernel, nz), out_shape=jax.ShapeDty...]
where the time goes in v3:
time: 146 us
  Pallas kernels  143 us (98%)
  local copies, waits for them, and re-layouts  1.67 us (1%)
    pallas_call x1, Pallas kernels, ring_device(): pl.pallas_call(functools.partial(ring_kernel, nz), out_shape=jax.ShapeDty...  143 us

profile of v3, /device:TPU:0, one launch (start us, length us, event | category | flops | bytes accessed | tf_op | source)
XLA Modules:
  0.0 145.8 jit_solution(15819580501133677648)
XLA Ops:
  0.0 0.1 broadcast_multiply_fusion.1
  0.2 1.3 sine_multiply_fusion
  1.4 142.7 %shard_map.109 = bf16[64,2048]{1,0:T(8,128)(2,1)} custom-call(bf16[64,2048]{1,0:T(8,128)(2,1)} %res_ref.1, bf16[256,512]{1,0:T(8,128)(2,1)} %q_ref.1, bf16[256,128]{1,0:T(8,128)(2,1)} %k_ref.1, bf16[256,128]{1,0:T(8,128)(2,1)} %v_ref.1, f32[256,128]{1,0:T(8,128)} %get-tuple-element.6.cos_ref, f32[256,128]{1,0:T(8,128)} %get-tuple-element.5.sin_ref, ...), custom_call_target="tpu_custom_call" | custom-call | tf_op jit(solution)/shard_map/pallas_call | solution.py:523
  144.2 1.7 %copy.13 = bf16[64,2048]{1,0:T(8,128)(2,1)} copy(bf16[64,2048]{1,0:T(8,128)(2,1)} %shard_map.109) | data formatting | bytes 524288
  (3 shorter events, 0.0 us)

commit v4 on v3

--- a/solution.py
+++ b/solution.py
@@ -417,7 +417,7 @@
     cols_each = d_all.shape[2]
 
     def tile(i, carry):
-        t = near(i)
+        t = near(jnp.where(i == 1, 2, jnp.where(i == 2, 1, i)))
 
         @pl.when(i == nz - 2)
         def _():
@@ -435,15 +435,16 @@
         for j in range(2):
             core_ops(t, j).start()
 
-        @pl.when(i > 1)
+        @pl.when(i == 2)
         def _():
-            y_stage(near(i - 1))
+            y_stage(near(2))
 
         return carry
 
     lax.fori_loop(0, nz, tile, 0)
 
-    y_stage(near(nz - 1))
+    y_stage(near(3))
+    y_stage(near(1))
     y_stage(z)
 
     def summed_tile(t):
@@ -452,14 +453,14 @@
     def z_op(i):
         return rc(z_out.at[i], z_in.at[z], z_s.at[i], z_r.at[z], at_z(near(i)))
 
-    for i in range(1, nz):
+    for i in (2, 3, 1):
         t = near(i)
         y_op(t).wait_recv()
         z_out[i] = summed_tile(t).astype(bf16)
         z_op(i).start()
     y_op(z).wait_recv()
     fed = summed_tile(z)
-    for i in range(1, nz):
+    for i in (2, 3, 1):
         t = near(i)
         rc(z_out.at[i], z_in.at[t], z_s.at[i], z_r.at[t], at_z(t)).wait_recv()
         fed = fed + z_in[t].astype(f32)

time: 146 us -> 145 us (level)
  no operation moved by 1% of the time
where the time goes in v4:
time: 145 us
  Pallas kernels  142 us (98%)
  local copies, waits for them, and re-layouts  1.67 us (1%)
    pallas_call x1, Pallas kernels, ring_device(): pl.pallas_call(functools.partial(ring_kernel, nz), out_shape=jax.ShapeDty...  142 us

profile of v4, /device:TPU:0, one launch (start us, length us, event | category | flops | bytes accessed | tf_op | source)
XLA Modules:
  0.0 145.0 jit_solution(7679772307081272460)
XLA Ops:
  0.0 0.1 broadcast_multiply_fusion.1
  0.2 1.3 sine_multiply_fusion
  1.4 141.9 %shard_map.109 = bf16[64,2048]{1,0:T(8,128)(2,1)} custom-call(bf16[64,2048]{1,0:T(8,128)(2,1)} %res_ref.1, bf16[256,512]{1,0:T(8,128)(2,1)} %q_ref.1, bf16[256,128]{1,0:T(8,128)(2,1)} %k_ref.1, bf16[256,128]{1,0:T(8,128)(2,1)} %v_ref.1, f32[256,128]{1,0:T(8,128)} %get-tuple-element.6.cos_ref, f32[256,128]{1,0:T(8,128)} %get-tuple-element.5.sin_ref, ...), custom_call_target="tpu_custom_call" | custom-call | tf_op jit(solution)/shard_map/pallas_call | solution.py:524
  143.3 1.7 %copy.13 = bf16[64,2048]{1,0:T(8,128)(2,1)} copy(bf16[64,2048]{1,0:T(8,128)(2,1)} %shard_map.109) | data formatting | bytes 524288
  (3 shorter events, 0.0 us)
